TPU v7x, 32 devices: a whole 2x2x4 slice. The times are simulated.
32 devices in a mesh: rep: 2 (over x), fs: 8 (over z, y), tp: 2 (over core).
Axes of the slice: x: 2, y: 2, z: 4, core: 2. Of those that a mesh axis runs over, the one named last changes fastest.
Arguments:
- resid: bfloat16 [4096, 2048], P(('rep', 'fs'), 'tp'), may hold values from -6 to 6
- norm_gains: float32 [3, 2048], replicated, may hold values from 0.1 to 1.9
- gate_one: bfloat16 [2048, 5632], P('fs', 'tp'), may hold values from -0.125 to 0.125
- up_one: bfloat16 [2048, 5632], P('fs', 'tp'), may hold values from -0.125 to 0.125
- down_one: bfloat16 [5632, 2048], P('tp', 'fs'), may hold values from -0.109375 to 0.109375
- proj_u: bfloat16 [2048, 1024], P('fs', 'tp'), may hold values from -0.125 to 0.125
- proj_v: bfloat16 [2048, 1024], P('fs', 'tp'), may hold values from -0.125 to 0.125
- spatial: bfloat16 [8, 128, 128], P('tp'), may hold values from -0.5 to 0.5
- spatial_bias: float32 [8, 128], P('tp'), may hold values from 0.1 to 1.9
- mix_gain: float32 [1024], P('tp'), may hold values from 0.1 to 1.9
- head_gain: float32 [1024], P('tp'), may hold values from 0.1 to 1.9
- proj_out: bfloat16 [1024, 2048], P('tp', 'fs'), may hold values from -0.25 to 0.25
- gate_two: bfloat16 [2048, 5632], P('fs', 'tp'), may hold values from -0.125 to 0.125
- up_two: bfloat16 [2048, 5632], P('fs', 'tp'), may hold values from -0.125 to 0.125
- down_two: bfloat16 [5632, 2048], P('tp', 'fs'), may hold values from -0.109375 to 0.109375
Outputs:
- layer_out: bfloat16 [4096, 2048], P(('rep', 'fs'), 'tp')
All inputs are finite; a program needn't handle non-finite values.
Results may differ from a plain program's by a relative error of at most 0.019.
Values may be sent and summed in bfloat16 or wider, within the bound.
A program may use at most 128 MiB of HBM per device.

v0:
```python
import functools

import jax
import jax.numpy as jnp
from jax import lax
from jax.experimental import pallas as pl
from jax.experimental.pallas import tpu as pltpu
from jax.sharding import PartitionSpec as P


HEAD_DIM = 128
BLOCK = 128
SPAN = 64


def rms_scale(values, gain):
    return values * lax.rsqrt(jnp.mean(values * values, axis=-1, keepdims=True) + 1e-06) * gain


def normalized(stream, gain):
    whole = lax.all_gather(stream, "tp", axis=1, tiled=True).astype(jnp.float32)
    return rms_scale(whole, gain).astype(jnp.bfloat16)


def accumulate(left, piece):
    return jnp.dot(left, piece, preferred_element_type=jnp.float32)


def folders(normed):

    def single(total, piece, start):
        return accumulate(normed, piece)

    def double(totals, pieces, start):
        return (accumulate(normed, pieces[0]), accumulate(normed, pieces[1]))

    return (single, double)


def ffn_inputs(normed, first_weight, second_weight):
    empty = jnp.zeros((normed.shape[0], first_weight.shape[1]), jnp.float32)
    single, _ = folders(normed)
    result = (
        single(empty, lax.all_gather(first_weight, "fs", axis=0, tiled=True), jnp.int32(0)),
        single(empty, lax.all_gather(second_weight, "fs", axis=0, tiled=True), jnp.int32(0)),
    )
    return result


def mixer_inputs(normed, first_weight, second_weight):
    empty = jnp.zeros((normed.shape[0], first_weight.shape[1]), jnp.float32)
    single, _ = folders(normed)
    result = (
        single(empty, lax.all_gather(first_weight, "fs", axis=0, tiled=True), jnp.int32(0)),
        single(empty, lax.all_gather(second_weight, "fs", axis=0, tiled=True), jnp.int32(0)),
    )
    return result


LANE = 128
MESH = pl.DeviceIdType.MESH
VMEM = pltpu.VMEM


def flip(value, bit):
    return value + bit - 2 * bit * lax.rem(lax.div(value, jnp.int32(bit)), 2)


def xor(value, mask):
    for bit in (1, 2, 4):
        if mask & bit:
            value = flip(value, bit)
    return value


class Place:
    def __init__(self):
        self.rep, self.fs, self.tp = (lax.axis_index(name) for name in ("rep", "fs", "tp"))
        self.y = lax.rem(self.fs, 2)
        self.z = lax.rem(lax.div(self.fs, jnp.int32(2)), 2)
        self.x_peer = {"rep": 1 - self.rep}
        self.y_peer = {"fs": flip(self.fs, 1)}
        self.z_peer = {"fs": flip(self.fs, 2)}
        self.sibling = {"tp": 1 - self.tp}

    def member(self, mask):
        return xor(4 * self.rep + 2 * self.y + self.z, mask)

    def barrier(self):
        semaphore = pltpu.get_barrier_semaphore()
        peers = [{"fs": xor(self.fs, mask)} for mask in range(1, 8)]
        peers += [self.x_peer, self.sibling]
        for peer in peers:
            pl.semaphore_signal(semaphore, inc=1, device_id=peer, device_id_type=MESH)
        pl.semaphore_wait(semaphore, len(peers))


def remote(src, dst, send, recv, peer):
    return pltpu.make_async_remote_copy(
        src_ref=src, dst_ref=dst, send_sem=send, recv_sem=recv,
        device_id=peer, device_id_type=MESH,
    )


def rows_at(index, size):
    return pl.ds(pl.multiple_of(index * size, size), size)


class Shares:
    def __init__(self, units):
        self.tiles = units // LANE // 2
        self.most = -(-self.tiles // 4)
        self.missing = 4 * self.most - self.tiles
        self.base = (self.most - (1 if self.missing else 0)) * LANE
        self.extra = LANE if self.missing else 0
        self.slot = self.most * LANE

    def of(self, place, quarter, core):
        late = 4 - self.missing
        before = jnp.where(
            core == 0, jnp.maximum(quarter - late, 0), jnp.minimum(quarter, self.missing)
        )
        long = jnp.where(core == 0, quarter < late, quarter >= self.missing)
        start = place.rep * self.tiles + quarter * self.most - before
        return start * LANE, long


class Weights:
    def __init__(self, place, shares, shards, whole, sems):
        self.place, self.shares, self.shards, self.whole = place, shares, shards, whole
        self.send_sem, self.recv_sem, self.pass_send, self.pass_recv, self.local = sems
        self.kinds = 6 if shares.extra else 3
        self.quarter = lax.rem(place.fs, 4)

    def source(self, kind, start):
        shares, which = self.shares, kind % 3
        first = start + (shares.base if kind >= 3 else 0)
        size = shares.extra if kind >= 3 else shares.base
        ref = self.shards[which]
        first = jnp.minimum(first, ref.shape[0 if which == 2 else 1] - size)
        cut = pl.ds(pl.multiple_of(first, LANE), size)
        return ref.at[cut, :] if which == 2 else ref.at[:, cut]

    def target(self, kind, owner, core):
        shares, which = self.shares, kind % 3
        first = core * shares.slot + (shares.base if kind >= 3 else 0)
        size = shares.extra if kind >= 3 else shares.base
        cut = pl.ds(pl.multiple_of(first, LANE), size)
        ref = self.whole[which]
        if which == 2:
            return ref.at[cut, rows_at(owner, self.shards[2].shape[1])]
        return ref.at[rows_at(owner, self.shards[which].shape[0]), cut]

    def when(self, kind, long, action):
        if kind >= 3:
            pl.when(long)(action)
        else:
            action()

    def out(self, kind, mask):
        peer = xor(self.place.fs, mask)
        start, long = self.shares.of(self.place, lax.rem(peer, 4), self.place.tp)
        return long, remote(
            self.source(kind, start),
            self.target(kind, self.place.fs, self.place.tp),
            self.send_sem.at[kind, mask],
            self.recv_sem.at[kind, mask],
            {"fs": peer},
        )

    def start(self, pieces):
        for kind, mask in pieces:
            long, copy = self.out(kind, mask)
            self.when(kind, long, copy.start)

    def own(self):
        start, long = self.shares.of(self.place, self.quarter, self.place.tp)
        for kind in range(self.kinds):
            source = self.source(kind, start)
            target = self.target(kind, self.place.fs, self.place.tp)
            here = pltpu.make_async_copy(source, target, self.local.at[kind])
            there = self.passed(kind, 0, source)

            def begin(here=here, there=there):
                here.start()
                there.start()

            self.when(kind, long, begin)

    def passed(self, kind, mask, source=None):
        target = self.target(kind, xor(self.place.fs, mask), self.place.tp)
        return remote(
            target if source is None else source,
            target,
            self.pass_send.at[kind, mask],
            self.pass_recv.at[kind, mask],
            self.place.sibling,
        )

    def blank(self):
        shares = self.shares
        if not shares.extra:
            return
        for core in range(2):
            _, long = shares.of(self.place, self.quarter, core)
            cut = pl.ds(core * shares.slot + shares.base, shares.extra)

            def clear(cut=cut):
                for ref in self.whole[:2]:
                    ref[:, cut] = jnp.zeros((ref.shape[0], shares.extra), ref.dtype)
                down = self.whole[2]
                down[cut, :] = jnp.zeros((shares.extra, down.shape[1]), down.dtype)

            pl.when(jnp.logical_not(long))(clear)

    def forward(self, pieces):
        _, long = self.shares.of(self.place, self.quarter, self.place.tp)
        for kind, mask in pieces:
            def step(kind=kind, mask=mask):
                self.out(kind, mask)[1].wait_recv()
                self.passed(kind, mask).start()

            self.when(kind, long, step)

    def finish(self):
        _, long = self.shares.of(self.place, self.quarter, self.place.tp)
        _, other = self.shares.of(self.place, self.quarter, 1 - self.place.tp)
        start, _ = self.shares.of(self.place, self.quarter, self.place.tp)
        for kind in range(self.kinds):
            here = pltpu.make_async_copy(
                self.source(kind, start),
                self.target(kind, self.place.fs, self.place.tp),
                self.local.at[kind],
            )
            self.when(kind, long, here.wait)
            for mask in range(8):
                def arrived(kind=kind, mask=mask):
                    target = self.target(kind, xor(self.place.fs, mask), 1 - self.place.tp)
                    remote(
                        target, target, self.pass_send.at[kind, mask],
                        self.pass_recv.at[kind, mask], self.place.sibling,
                    ).wait_recv()

                self.when(kind, other, arrived)

    def drain(self):
        _, long = self.shares.of(self.place, self.quarter, self.place.tp)
        start, _ = self.shares.of(self.place, self.quarter, self.place.tp)
        for kind in range(self.kinds):
            for mask in range(8):
                if mask:
                    sent, copy = self.out(kind, mask)
                    self.when(kind, sent, copy.wait_send)
                source = self.source(kind, start) if mask == 0 else None
                self.when(kind, long, self.passed(kind, mask, source).wait_send)


class Gather:
    def __init__(self, place, tokens, cut, send, recv):
        self.place, self.tokens, self.cut = place, tokens, cut
        self.send, self.recv = send, recv
        self.half = tokens.shape[0] // 8

    def copy(self, index):
        place, width = self.place, self.tokens.shape[1]
        left, right = pl.ds(0, self.cut), pl.ds(self.cut, width - self.cut)
        mask, columns, peer = (
            (0, pl.ds(0, width), place.z_peer),
            (0, pl.ds(0, width), place.y_peer),
            (1, pl.ds(0, width), place.y_peer),
            (0, pl.ds(0, width), place.x_peer),
            (1, pl.ds(0, width), place.x_peer),
            (2, left, place.x_peer),
            (3, left, place.x_peer),
            (4, right, place.y_peer),
            (5, right, place.y_peer),
        )[index]
        block = self.tokens.at[rows_at(place.member(mask), self.half), columns]
        return remote(block, block, self.send.at[index], self.recv.at[index], peer)

    def arrival(self, index):
        place, width = self.place, self.tokens.shape[1]
        left, right = pl.ds(0, self.cut), pl.ds(self.cut, width - self.cut)
        mask, columns = (
            (1, pl.ds(0, width)),
            (2, pl.ds(0, width)),
            (3, pl.ds(0, width)),
            (4, pl.ds(0, width)),
            (5, pl.ds(0, width)),
            (6, left),
            (7, left),
            (6, right),
            (7, right),
        )[index]
        block = self.tokens.at[rows_at(place.member(mask), self.half), columns]
        remote(block, block, self.send.at[index], self.recv.at[index], place.x_peer).wait_recv()


class Scatter:
    def __init__(self, place, part, cut, relay, from_x, from_y, send_z, from_z, send, recv):
        self.place, self.part, self.cut = place, part, cut
        self.relay, self.from_x, self.from_y = relay, from_x, from_y
        self.send_z, self.from_z = send_z, from_z
        self.send, self.recv = send, recv
        self.half = part.shape[0] // 8
        width = part.shape[1]
        self.left, self.right = pl.ds(0, cut), pl.ds(cut, width - cut)

    def block(self, turn, mask):
        return rows_at(self.place.member(2 * mask + 1 - turn), self.half)

    def copy(self, turn, index):
        place = self.place
        mask, columns, target, peer = (
            (3, self.left, self.relay, place.x_peer),
            (3, self.right, self.relay, place.y_peer),
            (2, self.left, self.from_x, place.x_peer),
            (1, self.right, self.from_y, place.y_peer),
            (1, self.left, self.from_y, place.y_peer),
            (2, self.right, self.from_x, place.x_peer),
        )[index]
        return remote(
            self.part.at[self.block(turn, mask), columns],
            target.at[pl.ds(turn * self.half, self.half), columns],
            self.send.at[turn, index],
            self.recv.at[turn, index],
            peer,
        )

    def add(self, turn, index):
        columns, mask = ((self.left, 1), (self.right, 2))[index]
        self.copy(turn, index).wait_recv()
        rows = self.block(turn, mask)
        got = self.relay[pl.ds(turn * self.half, self.half), columns]
        mine = self.part[rows, columns]
        total = mine.astype(jnp.float32) + got.astype(jnp.float32)
        self.part[rows, columns] = total.astype(self.part.dtype)
        self.copy(turn, 4 + index).start()

    def total(self, turn):
        for index in range(2, 6):
            self.copy(turn, index).wait_recv()
        rows = pl.ds(turn * self.half, self.half)
        result = self.part[self.block(turn, 0), :].astype(jnp.float32)
        result = result + self.from_x[rows, :].astype(jnp.float32)
        return result + self.from_y[rows, :].astype(jnp.float32)

    def z_copy(self):
        return remote(
            self.send_z, self.from_z, self.send.at[2, 0], self.recv.at[2, 0], self.place.z_peer
        )

    def drain(self):
        for turn in range(2):
            for index in range(6):
                self.copy(turn, index).wait_send()
        self.z_copy().wait_send()


def product(left, right):
    return jnp.dot(left, right, preferred_element_type=jnp.float32)


def ffn_stage(place, gather, weights, scatter, early):
    kinds = weights.kinds
    near, far = (1, 2, 3), (4, 5, 6, 7)
    rest = [(kind, mask) for kind in range(kinds) for mask in far + near]
    rest = [piece for piece in rest if piece not in early]
    for index in (0, 1, 3):
        gather.copy(index).start()
    third = len(rest) // 3
    weights.start(rest[:third])
    gather.arrival(0)
    gather.copy(2).start()
    gather.copy(4).start()
    weights.start(rest[third:])
    for index, relays in ((1, 5), (3, 7), (2, 6), (4, 8)):
        gather.arrival(index)
        gather.copy(relays).start()
    weights.forward(early + rest)
    for index in range(5, 9):
        gather.arrival(index)
    weights.finish()
    gate, up, down = weights.whole
    size = 2 * gather.half

    def quadrant(step, carry):
        @pl.when(step == 3)
        def relay():
            scatter.add(0, 0)
            scatter.add(0, 1)

        mask = 3 - step
        rep = lax.rem(place.rep + lax.div(mask, jnp.int32(2)), 2)
        y = lax.rem(place.y + lax.rem(mask, 2), 2)
        rows = rows_at(2 * rep + y, size)
        tokens = gather.tokens[rows, :]
        hidden = (
            jax.nn.silu(product(tokens, gate[...])) * product(tokens, up[...])
        ).astype(jnp.bfloat16)
        scatter.part[rows, :] = product(hidden, down[...]).astype(jnp.bfloat16)

        for which, indices in ((0, (0, 1)), (1, (2,)), (2, (3,))):
            def send(indices=indices):
                for turn in range(2):
                    for index in indices:
                        scatter.copy(turn, index).start()

            pl.when(step == which)(send)
        return carry

    lax.fori_loop(0, 4, quadrant, jnp.int32(0))
    scatter.add(1, 0)
    scatter.add(1, 1)
    scatter.send_z[...] = scatter.total(0).astype(jnp.bfloat16)
    scatter.z_copy().start()
    result = scatter.total(1)
    scatter.z_copy().wait_recv()
    return result + scatter.from_z[...].astype(jnp.float32)


def ffn_scratch(half, width, shares):
    token = lambda rows: VMEM((rows * half, width), jnp.bfloat16)
    sems = pltpu.SemaphoreType.DMA
    kinds = 6 if shares.extra else 3
    return [
        token(8),
        VMEM((width, 2 * shares.slot), jnp.bfloat16),
        VMEM((width, 2 * shares.slot), jnp.bfloat16),
        VMEM((2 * shares.slot, width), jnp.bfloat16),
        token(8), token(2), token(2), token(2), token(1), token(1),
        sems((9,)), sems((9,)),
        sems((kinds, 8)), sems((kinds, 8)), sems((kinds, 8)), sems((kinds, 8)), sems((kinds,)),
        sems((3, 6)), sems((3, 6)),
    ]


def ffn_parts(place, shares, shards, scratch, cut):
    (tokens, gate, up, down, part, relay, from_x, from_y, send_z, from_z,
     ag_send, ag_recv, w_send, w_recv, p_send, p_recv, w_local, rs_send, rs_recv) = scratch
    gather = Gather(place, tokens, cut, ag_send, ag_recv)
    weights = Weights(
        place, shares, shards, (gate, up, down), (w_send, w_recv, p_send, p_recv, w_local)
    )
    scatter = Scatter(
        place, part, cut, relay, from_x, from_y, send_z, from_z, rs_send, rs_recv
    )
    return gather, weights, scatter


FAR_GATE = [(0, mask) for mask in (4, 5, 6, 7)]
FAR_UP = [(1, mask) for mask in (4, 5, 6, 7)]


def kernel_one(shares, cut, stream, gain, gate, up, down, out, mine, send, recv, local, *scratch):
    place = Place()
    gather, weights, scatter = ffn_parts(place, shares, (gate, up, down), scratch, cut)
    half, _ = out.shape
    share = stream.shape[1]
    place.barrier()
    columns = rows_at(place.tp, share)
    there = remote(
        stream.at[rows_at(1 - place.tp, half), :], mine.at[:, columns],
        send.at[0], recv.at[0], place.sibling,
    )
    here = pltpu.make_async_copy(
        stream.at[rows_at(place.tp, half), :], mine.at[:, columns], local.at[0]
    )
    there.start()
    here.start()
    weights.start(FAR_GATE)
    weights.own()
    weights.blank()
    here.wait()
    there.wait_recv()
    normed = rms_scale(mine[...].astype(jnp.float32), gain[...])
    gather.tokens[rows_at(place.member(0), half), :] = normed.astype(jnp.bfloat16)
    total = ffn_stage(place, gather, weights, scatter, FAR_GATE)
    out[...] = (mine[...].astype(jnp.float32) + 0.5 * total).astype(jnp.bfloat16)
    there.wait_send()
    for index in range(9):
        gather.copy(index).wait_send()
    weights.drain()
    scatter.drain()


def kernel_two(
    shares, cut, first, gains, proj_u, proj_v, proj_out, spatial, bias, mix_gain, head_gain,
    gate, up, down, out, pu, pv, po, mixed_rows, gated, terms, other, second, result,
    send, recv, local, *scratch
):
    place = Place()
    gather, weights, scatter = ffn_parts(place, shares, (gate, up, down), scratch, cut)
    half, _ = first.shape
    share = out.shape[1]
    fetch = [
        pltpu.make_async_copy(source, target, local.at[index])
        for index, (source, target) in enumerate(((proj_u, pu), (proj_v, pv), (proj_out, po)))
    ]
    for copy in fetch:
        copy.start()
    place.barrier()
    weights.start(FAR_GATE + FAR_UP)
    weights.own()
    weights.blank()
    own, sibling = rows_at(place.tp, half), rows_at(1 - place.tp, half)
    normed = rms_scale(first[...].astype(jnp.float32), gains[0:1, :])
    mixed_rows[own, :] = normed.astype(jnp.bfloat16)
    trade = remote(
        mixed_rows.at[own, :], mixed_rows.at[own, :], send.at[0], recv.at[0], place.sibling
    )
    trade.start()
    for copy in fetch:
        copy.wait()
    trade_in = remote(
        mixed_rows.at[sibling, :], mixed_rows.at[sibling, :], send.at[0], recv.at[0], place.sibling
    )
    trade_in.wait_recv()
    row = lax.broadcasted_iota(jnp.int32, (BLOCK, BLOCK), 0) // SPAN
    column = lax.broadcasted_iota(jnp.int32, (BLOCK, BLOCK), 1) // SPAN
    causal = row >= column
    u_part = jax.nn.gelu(product(mixed_rows[...], pu[...]))
    v_part = jax.nn.gelu(product(mixed_rows[...], pv[...]))
    for head in range(spatial.shape[0]):
        at = slice(head * HEAD_DIM, (head + 1) * HEAD_DIM)
        matrix = jnp.where(causal, spatial[head], jnp.zeros_like(spatial[head]))
        for start in range(0, 2 * half, BLOCK):
            rows = slice(start, start + BLOCK)
            value = v_part[rows, at]
            centred = value - jnp.mean(value, axis=-1, keepdims=True)
            spread = jnp.mean(jnp.square(centred), axis=-1, keepdims=True)
            vn = (centred * lax.rsqrt(spread + 1e-05) * mix_gain[:, at]).astype(jnp.bfloat16)
            mixed = product(matrix, vn) + bias[:, head : head + 1]
            gated[rows, at] = rms_scale(u_part[rows, at] * mixed, head_gain[:, at]).astype(
                jnp.bfloat16
            )
    for part in range(po.shape[0]):
        at = pl.ds(part * po.shape[2], po.shape[2])
        terms[:, at] = product(gated[...], po[part]).astype(jnp.bfloat16)
    swap = remote(terms.at[sibling, :], other, send.at[1], recv.at[1], place.sibling)
    swap.start()
    swap.wait_recv()
    branch = terms[own, :].astype(jnp.float32) + other[...].astype(jnp.float32)
    second[...] = (first[...].astype(jnp.float32) + branch).astype(jnp.bfloat16)
    normed = rms_scale(second[...].astype(jnp.float32), gains[1:2, :])
    gather.tokens[rows_at(place.member(0), half), :] = normed.astype(jnp.bfloat16)
    total = ffn_stage(place, gather, weights, scatter, FAR_GATE + FAR_UP)
    result[...] = (second[...].astype(jnp.float32) + 0.5 * total).astype(jnp.bfloat16)
    there = remote(
        result.at[:, rows_at(1 - place.tp, share)], out.at[own, :],
        send.at[2], recv.at[2], place.sibling,
    )
    there.start()
    here = pltpu.make_async_copy(
        result.at[:, rows_at(place.tp, share)], out.at[own, :], local.at[0]
    )
    here.start()
    trade.wait_send()
    swap.wait_send()
    for index in range(9):
        gather.copy(index).wait_send()
    weights.drain()
    scatter.drain()
    there.wait_send()
    here.wait()
    remote(
        result.at[:, rows_at(1 - place.tp, share)], out.at[sibling, :],
        send.at[2], recv.at[2], place.sibling,
    ).wait_recv()


ANY = pl.BlockSpec(memory_space=pl.ANY)
WHOLE = pl.BlockSpec(memory_space=pltpu.VMEM)


def params(collective_id):
    return pltpu.CompilerParams(
        collective_id=collective_id, has_side_effects=True, vmem_limit_bytes=62 * 2**20
    )


def estimate(units, width, tokens):
    return pl.CostEstimate(
        flops=6 * tokens * units * width, bytes_accessed=64 * units * width, transcendentals=0
    )


def first_block(stream, gain, gate_weight, up_weight, down_weight):
    half, width = stream.shape[0] // 2, stream.shape[1] * lax.axis_size("tp")
    shares = Shares(gate_weight.shape[1])
    sems = pltpu.SemaphoreType.DMA
    return pl.pallas_call(
        functools.partial(kernel_one, shares, width // 2),
        out_shape=jax.ShapeDtypeStruct((half, width), jnp.bfloat16),
        in_specs=[ANY, WHOLE, ANY, ANY, ANY],
        out_specs=WHOLE,
        scratch_shapes=[
            VMEM((half, width), jnp.bfloat16), sems((1,)), sems((1,)), sems((1,)),
        ] + ffn_scratch(half, width, shares),
        compiler_params=params(1),
        cost_estimate=estimate(gate_weight.shape[1], width, stream.shape[0]),
    )(stream, gain[None], gate_weight, up_weight, down_weight)


def second_block(first, gains, projections, mixing, weights):
    half, width = first.shape
    shares = Shares(weights[0].shape[1])
    sems = pltpu.SemaphoreType.DMA
    channels = projections[0].shape[1]
    bf16 = jnp.bfloat16
    return pl.pallas_call(
        functools.partial(kernel_two, shares, width // 2),
        out_shape=jax.ShapeDtypeStruct((2 * half, width // 2), bf16),
        in_specs=[WHOLE, WHOLE, ANY, ANY, ANY, WHOLE, WHOLE, WHOLE, WHOLE, ANY, ANY, ANY],
        out_specs=ANY,
        scratch_shapes=[
            VMEM((width, channels), bf16),
            VMEM((width, channels), bf16),
            VMEM(projections[2].shape, bf16),
            VMEM((2 * half, width), bf16),
            VMEM((2 * half, channels), bf16),
            VMEM((2 * half, width), bf16),
            VMEM((half, width), bf16),
            VMEM((half, width), bf16),
            VMEM((half, width), bf16),
            sems((3,)), sems((3,)), sems((3,)),
        ] + ffn_scratch(half, width, shares),
        compiler_params=params(2),
        cost_estimate=estimate(weights[0].shape[1], width, 2 * half),
    )(first, gains, *projections, *mixing, *weights)


def cubes(stream, gate_weight):
    sizes = tuple(lax.axis_size(name) for name in ("rep", "fs", "tp"))
    rows, units = gate_weight.shape
    width = stream.shape[1] * 2
    return (
        sizes == (2, 8, 2)
        and stream.shape[0] % (2 * BLOCK) == 0
        and stream.shape[1] % (2 * LANE) == 0
        and units % (2 * LANE) == 0
        and units >= 16 * LANE
        and rows % 32 == 0
        and width * (6 * units // 8 + 22 * stream.shape[0] // 2 + 3 * 512) * 2 < 48 * 2**20
    )


def feed_forward(stream, gain, gate_weight, up_weight, down_weight):
    normed = normalized(stream, gain)
    gate, up_part = ffn_inputs(normed, gate_weight, up_weight)
    hidden = (jax.nn.silu(gate) * up_part).astype(jnp.bfloat16)
    terms = jnp.dot(
        hidden,
        lax.all_gather(down_weight, "fs", axis=1, tiled=True),
        preferred_element_type=jnp.float32,
    )
    return lax.psum_scatter(
        terms.astype(jnp.bfloat16), "tp", scatter_dimension=1, tiled=True
    ).astype(jnp.float32)


def body(
    resid,
    norm_gains,
    gate_one,
    up_one,
    down_one,
    proj_u,
    proj_v,
    spatial,
    spatial_bias,
    mix_gain,
    head_gain,
    proj_out,
    gate_two,
    up_two,
    down_two,
):
    if cubes(resid, gate_one):
        whole_u = lax.all_gather(proj_u, "fs", axis=0, tiled=True)
        whole_v = lax.all_gather(proj_v, "fs", axis=0, tiled=True)
        whole_out = lax.all_gather(proj_out, "fs", axis=0)
        first = first_block(resid, norm_gains[0], gate_one, up_one, down_one)
        return second_block(
            first, norm_gains[1:], (whole_u, whole_v, whole_out),
            (spatial, spatial_bias.T, mix_gain[None], head_gain[None]),
            (gate_two, up_two, down_two),
        )
    total = feed_forward(resid, norm_gains[0], gate_one, up_one, down_one)
    first = (resid.astype(jnp.float32) + 0.5 * total).astype(jnp.bfloat16)
    mnormed = normalized(first, norm_gains[1])
    u_part, v_part = mixer_inputs(mnormed, proj_u, proj_v)
    proj_out = lax.all_gather(proj_out, "fs", axis=1, tiled=True)
    rows = u_part.shape[0]
    seqs = rows // BLOCK
    local_heads = spatial.shape[0]
    gated_u = jax.nn.gelu(u_part).reshape(seqs, BLOCK, local_heads, HEAD_DIM)
    gated_v = jax.nn.gelu(v_part).reshape(seqs, BLOCK, local_heads, HEAD_DIM)
    centre = jnp.mean(gated_v, axis=-1, keepdims=True)
    spread = jnp.mean(jnp.square(gated_v - centre), axis=-1, keepdims=True)
    vn = (
        (gated_v - centre) * lax.rsqrt(spread + 1e-05) * mix_gain.reshape(local_heads, HEAD_DIM)
    ).astype(jnp.bfloat16)
    segment = jnp.arange(BLOCK) // SPAN
    causal = segment[:, None] >= segment[None, :]
    masked = jnp.where(causal[None], spatial, jnp.zeros_like(spatial))
    mixed = (
        jnp.einsum("hts,bshd->bthd", masked, vn, preferred_element_type=jnp.float32)
        + spatial_bias.T[None, :, :, None]
    )
    product = gated_u * mixed
    gated = (
        rms_scale(product, head_gain.reshape(local_heads, HEAD_DIM))
        .astype(jnp.bfloat16)
        .reshape(rows, local_heads * HEAD_DIM)
    )
    terms = jnp.dot(
        gated,
        proj_out,
        preferred_element_type=jnp.float32,
    )
    branch = lax.psum_scatter(
        terms.astype(jnp.bfloat16), "tp", scatter_dimension=1, tiled=True
    ).astype(jnp.float32)
    second = (first.astype(jnp.float32) + branch).astype(jnp.bfloat16)
    total = feed_forward(second, norm_gains[2], gate_two, up_two, down_two)
    return (second.astype(jnp.float32) + 0.5 * total).astype(jnp.bfloat16)


def solution(mesh):
    return jax.shard_map(
        body,
        mesh=mesh,
        in_specs=(
            P(("rep", "fs"), "tp"),
            P(),
            P("fs", "tp"),
            P("fs", "tp"),
            P("tp", "fs"),
            P("fs", "tp"),
            P("fs", "tp"),
            P("tp", None, None),
            P("tp", None),
            P("tp"),
            P("tp"),
            P("tp", "fs"),
            P("fs", "tp"),
            P("fs", "tp"),
            P("tp", "fs"),
        ),
        out_specs=P(("rep", "fs"), "tp"),
        check_vma=False,
    )
```

profile of v0, /device:TPU:9, one launch (start us, length us, event | category | flops | bytes accessed | tf_op | source)
XLA Modules:
  0.0 378.7 jit_solution(4248144343197830920)
XLA Ops:
  6.5 0.0 all-gather.5.cloned.1.call-start
  6.5 0.7 all-gather.5.cloned.1.call-update
  7.3 0.0 all-gather.7.cloned.1.call-start
  7.3 0.7 all-gather.7.cloned.1.call-update
  8.0 0.0 all-gather.9.cloned.1.call-start
  8.1 0.7 all-gather.9.cloned.1.call-update
  8.7 1.4 slice.6.gain
  10.1 1.4 slice.7.gains
  11.5 1.4 copy.16
  12.9 193.7 %shard_map.145.first = bf16[128,2048]{1,0:T(8,128)(2,1)} custom-call(bf16[256,1024]{1,0:T(8,128)(2,1)} %stream.1, f32[1,2048]{1,0:T(1,128)} %slice.6.gain, bf16[256,2816]{1,0:T(8,128)(2,1)} %gate.2, bf16[256,2816]{1,0:T(8,128)(2,1)} %up.2, bf16[2816,256]{1,0:T(8,128)(2,1)} %down.2), custom_call_target="tpu_custom_call" | custom-call | flops 8858370048 | bytes 369098752 | tf_op jit(solution)/shard_map/pallas_call | solution.py:592
  206.6 0.0 all-gather.5.cloned.1.call-done.proj_u
  206.6 0.0 all-gather.7.cloned.1.call-done.proj_v
  206.6 15.7 %all-gather.9.cloned.1.call-done = bf16[4096,256]{1,0:T(8,128)(2,1)} async-done(((bf16[512,256]{1,0:T(8,128)(2,1)}), bf16[4096,256]{1,0:T(8,128)(2,1)}) %all-gather.9.cloned.1.call-update) | async-done | bytes 2097168 | tf_op jit(solution)/shard_map/all_gather | solution.py:682
  222.4 147.9 %shard_map.146 = bf16[256,1024]{1,0:T(8,128)(2,1)} custom-call(bf16[128,2048]{1,0:T(8,128)(2,1)} %shard_map.145.first, f32[2,2048]{1,0:T(2,128)} %slice.7.gains, bf16[2048,512]{1,0:T(8,128)(2,1)} %all-gather.5.cloned.1.call-done.proj_u, bf16[2048,512]{1,0:T(8,128)(2,1)} %all-gather.7.cloned.1.call-done.proj_v, bf16[8,512,256]{2,1,0:T(8,128)(2,1)} %bitcast.5, ...), custom_call_target="tpu_custom_call" | custom-call | flops 8858370048 | bytes 369098752 | tf_op jit(solution)/shard_map/pallas_call | solution.py:611
  370.3 1.9 copy.18
Async XLA Ops:
  6.5 200.1 %all-gather.5.cloned.1.call-start = ((), (), s32[]{:S(2)}) async-start(), calls=%async_computation | async-start | bytes 2359296 | tf_op jit(solution)/shard_map/all_gather | solution.py:680
  7.3 199.4 %all-gather.7.cloned.1.call-start = ((), (), s32[]{:S(2)}) async-start(), calls=%async_computation.1 | async-start | bytes 2359296 | tf_op jit(solution)/shard_map/all_gather | solution.py:681
  8.0 214.4 %all-gather.9.cloned.1.call-start = ((), (), s32[]{:S(2)}) async-start(), calls=%async_computation.2 | async-start | bytes 2359296 | tf_op jit(solution)/shard_map/all_gather | solution.py:682
Sparse Core Ops, SparseCore 0:
  9.5 93.7 all-gather.4
  105.4 61.6 all-gather.6
  169.2 53.1 all-gather.8
where the time goes:
time: 383 us; the launch traced here: 379 us
  Pallas kernels  342 us (89%)
  waiting for transfers between devices  17.9 us (5%)
  between operations  13.1 us (3%)
  local copies, waits for them, and re-layouts  6.01 us (2%)
    pallas_call x1, Pallas kernels, first_block(): pl.pallas_call(functools.partial(kernel_one, shares, width // 2), out_sha...  194 us
    pallas_call x1, Pallas kernels, second_block(): pl.pallas_call(functools.partial(kernel_two, shares, width // 2), out_sha...  148 us
    all_gather x1, waiting for transfers between devices, body(): whole_out = lax.all_gather(proj_out, 'fs', axis=0)  15.7 us
  transfers between devices with their start and end apart: 3, of which 1 were waited for; matrix products, arithmetic and copies ran while one was open for 1% of the time, Pallas kernels for 51%

commit v1 on v0

--- a/solution.py
+++ b/solution.py
@@ -6,7 +6,6 @@
 from jax.experimental import pallas as pl
 from jax.experimental.pallas import tpu as pltpu
 from jax.sharding import PartitionSpec as P
-
 
 HEAD_DIM = 128
 BLOCK = 128
@@ -295,6 +294,10 @@
         block = self.tokens.at[rows_at(place.member(mask), self.half), columns]
         remote(block, block, self.send.at[index], self.recv.at[index], place.x_peer).wait_recv()
 
+    def drain(self):
+        for index in range(9):
+            self.copy(index).wait_send()
+
 
 class Scatter:
     def __init__(self, place, part, cut, relay, from_x, from_y, send_z, from_z, send, recv):
@@ -361,26 +364,29 @@
     return jnp.dot(left, right, preferred_element_type=jnp.float32)
 
 
-def ffn_stage(place, gather, weights, scatter, early):
-    kinds = weights.kinds
-    near, far = (1, 2, 3), (4, 5, 6, 7)
-    rest = [(kind, mask) for kind in range(kinds) for mask in far + near]
-    rest = [piece for piece in rest if piece not in early]
+def gather_start(gather):
     for index in (0, 1, 3):
         gather.copy(index).start()
-    third = len(rest) // 3
-    weights.start(rest[:third])
+
+
+def gather_near(gather):
     gather.arrival(0)
     gather.copy(2).start()
     gather.copy(4).start()
-    weights.start(rest[third:])
+
+
+def gather_relay(gather):
     for index, relays in ((1, 5), (3, 7), (2, 6), (4, 8)):
         gather.arrival(index)
         gather.copy(relays).start()
-    weights.forward(early + rest)
+
+
+def gather_finish(gather):
     for index in range(5, 9):
         gather.arrival(index)
-    weights.finish()
+
+
+def block_sums(place, gather, weights, scatter, soon, later):
     gate, up, down = weights.whole
     size = 2 * gather.half
 
@@ -389,6 +395,8 @@
         def relay():
             scatter.add(0, 0)
             scatter.add(0, 1)
+            for index in (0, 2, 3):
+                scatter.copy(1, index).start()
 
         mask = 3 - step
         rep = lax.rem(place.rep + lax.div(mask, jnp.int32(2)), 2)
@@ -400,18 +408,20 @@
         ).astype(jnp.bfloat16)
         scatter.part[rows, :] = product(hidden, down[...]).astype(jnp.bfloat16)
 
-        for which, indices in ((0, (0, 1)), (1, (2,)), (2, (3,))):
-            def send(indices=indices):
-                for turn in range(2):
-                    for index in indices:
-                        scatter.copy(turn, index).start()
+        for which, copies in ((0, ((0, 0), (0, 1), (1, 1))), (1, ((0, 2),)), (2, ((0, 3),))):
+            def send(copies=copies):
+                for turn, index in copies:
+                    scatter.copy(turn, index).start()
 
             pl.when(step == which)(send)
         return carry
 
     lax.fori_loop(0, 4, quadrant, jnp.int32(0))
+    gather.drain()
+    soon()
     scatter.add(1, 0)
     scatter.add(1, 1)
+    later()
     scatter.send_z[...] = scatter.total(0).astype(jnp.bfloat16)
     scatter.z_copy().start()
     result = scatter.total(1)
@@ -419,215 +429,290 @@
     return result + scatter.from_z[...].astype(jnp.float32)
 
 
-def ffn_scratch(half, width, shares):
-    token = lambda rows: VMEM((rows * half, width), jnp.bfloat16)
-    sems = pltpu.SemaphoreType.DMA
-    kinds = 6 if shares.extra else 3
-    return [
-        token(8),
-        VMEM((width, 2 * shares.slot), jnp.bfloat16),
-        VMEM((width, 2 * shares.slot), jnp.bfloat16),
-        VMEM((2 * shares.slot, width), jnp.bfloat16),
-        token(8), token(2), token(2), token(2), token(1), token(1),
-        sems((9,)), sems((9,)),
-        sems((kinds, 8)), sems((kinds, 8)), sems((kinds, 8)), sems((kinds, 8)), sems((kinds,)),
-        sems((3, 6)), sems((3, 6)),
-    ]
-
-
-def ffn_parts(place, shares, shards, scratch, cut):
-    (tokens, gate, up, down, part, relay, from_x, from_y, send_z, from_z,
-     ag_send, ag_recv, w_send, w_recv, p_send, p_recv, w_local, rs_send, rs_recv) = scratch
-    gather = Gather(place, tokens, cut, ag_send, ag_recv)
-    weights = Weights(
-        place, shares, shards, (gate, up, down), (w_send, w_recv, p_send, p_recv, w_local)
-    )
-    scatter = Scatter(
-        place, part, cut, relay, from_x, from_y, send_z, from_z, rs_send, rs_recv
-    )
-    return gather, weights, scatter
-
-
-FAR_GATE = [(0, mask) for mask in (4, 5, 6, 7)]
-FAR_UP = [(1, mask) for mask in (4, 5, 6, 7)]
-
-
-def kernel_one(shares, cut, stream, gain, gate, up, down, out, mine, send, recv, local, *scratch):
-    place = Place()
-    gather, weights, scatter = ffn_parts(place, shares, (gate, up, down), scratch, cut)
-    half, _ = out.shape
-    share = stream.shape[1]
-    place.barrier()
-    columns = rows_at(place.tp, share)
-    there = remote(
-        stream.at[rows_at(1 - place.tp, half), :], mine.at[:, columns],
-        send.at[0], recv.at[0], place.sibling,
-    )
-    here = pltpu.make_async_copy(
-        stream.at[rows_at(place.tp, half), :], mine.at[:, columns], local.at[0]
-    )
-    there.start()
-    here.start()
-    weights.start(FAR_GATE)
-    weights.own()
-    weights.blank()
-    here.wait()
-    there.wait_recv()
-    normed = rms_scale(mine[...].astype(jnp.float32), gain[...])
-    gather.tokens[rows_at(place.member(0), half), :] = normed.astype(jnp.bfloat16)
-    total = ffn_stage(place, gather, weights, scatter, FAR_GATE)
-    out[...] = (mine[...].astype(jnp.float32) + 0.5 * total).astype(jnp.bfloat16)
-    there.wait_send()
-    for index in range(9):
-        gather.copy(index).wait_send()
-    weights.drain()
-    scatter.drain()
-
-
-def kernel_two(
-    shares, cut, first, gains, proj_u, proj_v, proj_out, spatial, bias, mix_gain, head_gain,
-    gate, up, down, out, pu, pv, po, mixed_rows, gated, terms, other, second, result,
-    send, recv, local, *scratch
-):
-    place = Place()
-    gather, weights, scatter = ffn_parts(place, shares, (gate, up, down), scratch, cut)
-    half, _ = first.shape
-    share = out.shape[1]
-    fetch = [
-        pltpu.make_async_copy(source, target, local.at[index])
-        for index, (source, target) in enumerate(((proj_u, pu), (proj_v, pv), (proj_out, po)))
-    ]
-    for copy in fetch:
-        copy.start()
-    place.barrier()
-    weights.start(FAR_GATE + FAR_UP)
-    weights.own()
-    weights.blank()
+class Mixing:
+    SLOTS = tuple(
+        [("far", 0)]
+        + [("z", mask) for mask in (0, 4)]
+        + [("y", mask) for mask in (0, 4, 2, 6)]
+        + [("x", mask) for mask in (4, 2, 6, 1, 5, 3, 7)]
+    )
+
+    def __init__(self, place, shards, whole, send, recv, local):
+        self.place, self.shards, self.whole = place, shards, whole
+        self.send, self.recv, self.local = send, recv, local
+
+    def part(self, kind, half):
+        size = self.shards[kind].shape[0] // 2
+        return self.shards[kind].at[rows_at(half, size), :]
+
+    def target(self, kind, owner, half):
+        size = self.shards[kind].shape[0] // 2
+        if kind == 2:
+            return self.whole[2].at[owner, rows_at(half, size), :]
+        return self.whole[kind].at[rows_at(2 * owner + half, size), :]
+
+    def copy(self, kind, slot):
+        place = self.place
+        way, mask = self.SLOTS[slot]
+        peer = {
+            "far": {"fs": xor(place.fs, 4)},
+            "y": place.y_peer,
+            "z": place.z_peer,
+            "x": place.x_peer,
+        }[way]
+        target = self.target(kind, xor(place.fs, mask), place.rep)
+        source = target if mask else self.part(kind, place.rep)
+        return remote(source, target, self.send.at[kind, slot], self.recv.at[kind, slot], peer)
+
+    def start(self, slots):
+        for slot in slots:
+            for kind in range(3):
+                self.copy(kind, slot).start()
+
+    def arrive(self, slots):
+        place = self.place
+        for slot in slots:
+            way, mask = self.SLOTS[slot]
+            mask ^= {"far": 4, "y": 1, "z": 2, "x": 0}[way]
+            half = 1 - place.rep if way == "x" else place.rep
+            for kind in range(3):
+                target = self.target(kind, xor(place.fs, mask), half)
+                remote(
+                    target, target, self.send.at[kind, slot], self.recv.at[kind, slot],
+                    place.x_peer,
+                ).wait_recv()
+
+    def own(self):
+        copies = []
+        for kind in range(3):
+            size = self.shards[kind].shape[0]
+            target = (
+                self.whole[2].at[self.place.fs]
+                if kind == 2
+                else self.whole[kind].at[rows_at(self.place.fs, size), :]
+            )
+            copies.append(
+                pltpu.make_async_copy(self.shards[kind], target, self.local.at[kind])
+            )
+        return copies
+
+    def drain(self):
+        for slot in range(len(self.SLOTS)):
+            for kind in range(3):
+                self.copy(kind, slot).wait_send()
+
+
+def mix(place, first, normed_rows, projections, mixing, gated, terms, other, send, recv):
+    spatial, bias, mix_gain, head_gain = mixing
+    pu, pv, po = projections
+    half = first.shape[0]
     own, sibling = rows_at(place.tp, half), rows_at(1 - place.tp, half)
-    normed = rms_scale(first[...].astype(jnp.float32), gains[0:1, :])
-    mixed_rows[own, :] = normed.astype(jnp.bfloat16)
-    trade = remote(
-        mixed_rows.at[own, :], mixed_rows.at[own, :], send.at[0], recv.at[0], place.sibling
-    )
-    trade.start()
-    for copy in fetch:
-        copy.wait()
-    trade_in = remote(
-        mixed_rows.at[sibling, :], mixed_rows.at[sibling, :], send.at[0], recv.at[0], place.sibling
-    )
-    trade_in.wait_recv()
-    row = lax.broadcasted_iota(jnp.int32, (BLOCK, BLOCK), 0) // SPAN
-    column = lax.broadcasted_iota(jnp.int32, (BLOCK, BLOCK), 1) // SPAN
-    causal = row >= column
-    u_part = jax.nn.gelu(product(mixed_rows[...], pu[...]))
-    v_part = jax.nn.gelu(product(mixed_rows[...], pv[...]))
+    remote(
+        normed_rows.at[sibling, :], normed_rows.at[sibling, :], send.at[1], recv.at[1],
+        place.sibling,
+    ).wait_recv()
+    row = lax.broadcasted_iota(jnp.int32, (BLOCK, BLOCK), 0)
+    column = lax.broadcasted_iota(jnp.int32, (BLOCK, BLOCK), 1)
+    causal = lax.div(row, SPAN) >= lax.div(column, SPAN)
+    u_part = jax.nn.gelu(product(normed_rows[...], pu[...]))
+    v_part = jax.nn.gelu(product(normed_rows[...], pv[...]))
     for head in range(spatial.shape[0]):
         at = slice(head * HEAD_DIM, (head + 1) * HEAD_DIM)
         matrix = jnp.where(causal, spatial[head], jnp.zeros_like(spatial[head]))
+        shift = jnp.sum(
+            jnp.where(row == column, bias[head : head + 1, :], 0.0), axis=1, keepdims=True
+        )
         for start in range(0, 2 * half, BLOCK):
             rows = slice(start, start + BLOCK)
             value = v_part[rows, at]
             centred = value - jnp.mean(value, axis=-1, keepdims=True)
             spread = jnp.mean(jnp.square(centred), axis=-1, keepdims=True)
             vn = (centred * lax.rsqrt(spread + 1e-05) * mix_gain[:, at]).astype(jnp.bfloat16)
-            mixed = product(matrix, vn) + bias[:, head : head + 1]
+            mixed = product(matrix, vn) + shift
             gated[rows, at] = rms_scale(u_part[rows, at] * mixed, head_gain[:, at]).astype(
                 jnp.bfloat16
             )
     for part in range(po.shape[0]):
         at = pl.ds(part * po.shape[2], po.shape[2])
         terms[:, at] = product(gated[...], po[part]).astype(jnp.bfloat16)
-    swap = remote(terms.at[sibling, :], other, send.at[1], recv.at[1], place.sibling)
+    swap = remote(terms.at[sibling, :], other, send.at[2], recv.at[2], place.sibling)
     swap.start()
     swap.wait_recv()
     branch = terms[own, :].astype(jnp.float32) + other[...].astype(jnp.float32)
-    second[...] = (first[...].astype(jnp.float32) + branch).astype(jnp.bfloat16)
-    normed = rms_scale(second[...].astype(jnp.float32), gains[1:2, :])
-    gather.tokens[rows_at(place.member(0), half), :] = normed.astype(jnp.bfloat16)
-    total = ffn_stage(place, gather, weights, scatter, FAR_GATE + FAR_UP)
+    return first[...].astype(jnp.float32) + branch
+
+
+def near_pieces(kinds):
+    return [(kind, mask) for kind in kinds for mask in (1, 2, 3)]
+
+
+def far_pieces(kinds):
+    return [(kind, mask) for kind in kinds for mask in (4, 5, 6, 7)]
+
+
+def layer_kernel(shares, cuts, *refs):
+    (stream, gains, gate_one, up_one, down_one, proj_u, proj_v, spatial, bias, mix_gain,
+     head_gain, proj_out, gate_two, up_two, down_two, out) = refs[:16]
+    (mine, first, second, normed_rows, gated, terms, other, result, pu, pv, po,
+     tokens, part, relay, from_x, from_y, send_z, from_z) = refs[16:34]
+    send, recv, local, mix_send, mix_recv, mix_local = refs[34:40]
+    ag_send, ag_recv, rs_send, rs_recv = refs[40:44]
+    place = Place()
+    weights, gathers, scatters = [], [], []
+    for which, shards in enumerate(((gate_one, up_one, down_one), (gate_two, up_two, down_two))):
+        whole, sems = refs[44 + 8 * which : 47 + 8 * which], refs[47 + 8 * which : 52 + 8 * which]
+        weights.append(Weights(place, shares, shards, whole, sems))
+        gathers.append(Gather(place, tokens, cuts[2 * which], ag_send.at[which], ag_recv.at[which]))
+        scatters.append(
+            Scatter(place, part, cuts[2 * which + 1], relay, from_x, from_y, send_z, from_z,
+                    rs_send.at[which], rs_recv.at[which])
+        )
+    mixing = Mixing(place, (proj_u, proj_v, proj_out), (pu, pv, po), mix_send, mix_recv, mix_local)
+    half, _ = mine.shape
+    share = stream.shape[1]
+    place.barrier()
+
+    own, sibling = rows_at(place.tp, half), rows_at(1 - place.tp, half)
+    columns = rows_at(place.tp, share)
+    there = remote(
+        stream.at[sibling, :], mine.at[:, columns], send.at[0], recv.at[0], place.sibling
+    )
+    here = pltpu.make_async_copy(stream.at[own, :], mine.at[:, columns], local.at[0])
+    there.start()
+    here.start()
+    mixing.start((0, 1, 3))
+    one, two = weights
+    for copy in mixing.own():
+        copy.start()
+    here.wait()
+    there.wait_recv()
+    block = rows_at(place.member(0), half)
+    normed = rms_scale(mine[...].astype(jnp.float32), gains[0:1, :])
+    tokens[block, :] = normed.astype(jnp.bfloat16)
+    gather_start(gathers[0])
+    extras = (3, 4, 5) if shares.extra else ()
+    one.start(far_pieces((0,)))
+    one.own()
+    one.blank()
+    two.blank()
+    mixing.arrive((0,))
+    mixing.start((2, 4, 7))
+    one.start(far_pieces((1,)))
+    mixing.arrive((1, 3))
+    mixing.start((5, 8, 10))
+    gather_near(gathers[0])
+    mixing.arrive((2, 4))
+    mixing.start((6, 9, 11))
+    one.start(far_pieces((2,) + extras))
+    one.start(near_pieces((0, 1, 2) + extras))
+    gather_relay(gathers[0])
+    mixing.arrive((5, 6))
+    mixing.start((12, 13))
+    one.forward(far_pieces((0, 1, 2) + extras) + near_pieces((0, 1, 2) + extras))
+    gather_finish(gathers[0])
+    two.start(far_pieces((0,)))
+    one.finish()
+    total = block_sums(
+        place, gathers[0], one, scatters[0],
+        lambda: two.start(far_pieces((1,)) + [(kind, 2) for kind in (0, 1, 2)]),
+        lambda: two.start(
+            far_pieces((2,)) + [(kind, mask) for kind in (0, 1) for mask in (1, 3)]
+        ),
+    )
+    first[...] = (mine[...].astype(jnp.float32) + 0.5 * total).astype(jnp.bfloat16)
+
+    normed = rms_scale(first[...].astype(jnp.float32), gains[1:2, :])
+    normed_rows[own, :] = normed.astype(jnp.bfloat16)
+    trade = remote(
+        normed_rows.at[own, :], normed_rows.at[own, :], send.at[1], recv.at[1], place.sibling
+    )
+    trade.start()
+    two.own()
+    for copy in mixing.own():
+        copy.wait()
+    mixing.arrive(range(7, 14))
+    second[...] = mix(
+        place, first, normed_rows, (pu, pv, po), (spatial, bias, mix_gain, head_gain),
+        gated, terms, other, send, recv,
+    ).astype(jnp.bfloat16)
+    scatters[0].drain()
+    normed = rms_scale(second[...].astype(jnp.float32), gains[2:3, :])
+    tokens[block, :] = normed.astype(jnp.bfloat16)
+    gather_start(gathers[1])
+    gather_near(gathers[1])
+    two.start(far_pieces(extras) + [(2, 1), (2, 3)] + near_pieces(extras))
+    gather_relay(gathers[1])
+    two.forward(far_pieces((0, 1, 2) + extras) + near_pieces((0, 1, 2) + extras))
+    gather_finish(gathers[1])
+    two.finish()
+    total = block_sums(place, gathers[1], two, scatters[1], lambda: None, lambda: None)
     result[...] = (second[...].astype(jnp.float32) + 0.5 * total).astype(jnp.bfloat16)
-    there = remote(
+
+    last = remote(
         result.at[:, rows_at(1 - place.tp, share)], out.at[own, :],
-        send.at[2], recv.at[2], place.sibling,
-    )
-    there.start()
-    here = pltpu.make_async_copy(
+        send.at[3], recv.at[3], place.sibling,
+    )
+    last.start()
+    keep = pltpu.make_async_copy(
         result.at[:, rows_at(place.tp, share)], out.at[own, :], local.at[0]
     )
-    here.start()
+    keep.start()
+    there.wait_send()
     trade.wait_send()
-    swap.wait_send()
-    for index in range(9):
-        gather.copy(index).wait_send()
-    weights.drain()
-    scatter.drain()
-    there.wait_send()
-    here.wait()
+    remote(terms.at[sibling, :], other, send.at[2], recv.at[2], place.sibling).wait_send()
+    mixing.drain()
+    one.drain()
+    two.drain()
+    scatters[1].drain()
+    last.wait_send()
+    keep.wait()
     remote(
         result.at[:, rows_at(1 - place.tp, share)], out.at[sibling, :],
-        send.at[2], recv.at[2], place.sibling,
+        send.at[3], recv.at[3], place.sibling,
     ).wait_recv()
 
 
-ANY = pl.BlockSpec(memory_space=pl.ANY)
-WHOLE = pl.BlockSpec(memory_space=pltpu.VMEM)
-
-
-def params(collective_id):
-    return pltpu.CompilerParams(
-        collective_id=collective_id, has_side_effects=True, vmem_limit_bytes=62 * 2**20
-    )
-
-
-def estimate(units, width, tokens):
-    return pl.CostEstimate(
-        flops=6 * tokens * units * width, bytes_accessed=64 * units * width, transcendentals=0
-    )
-
-
-def first_block(stream, gain, gate_weight, up_weight, down_weight):
-    half, width = stream.shape[0] // 2, stream.shape[1] * lax.axis_size("tp")
-    shares = Shares(gate_weight.shape[1])
+def whole_layer(*args):
+    stream, gate, proj_u, proj_out = args[0], args[2], args[5], args[11]
+    half, width = stream.shape[0] // 2, 2 * stream.shape[1]
+    shares = Shares(gate.shape[1])
+    channels = proj_u.shape[1]
+    kinds = 6 if shares.extra else 3
+    parts = lax.axis_size("fs")
+    even, wide = width // 2, width // 8 * 6 // LANE * LANE
+    cuts = (wide, wide, wide, even)
     sems = pltpu.SemaphoreType.DMA
+    array = lambda *shape: VMEM(shape, jnp.bfloat16)
+    any_space, vmem = (pl.BlockSpec(memory_space=space) for space in (pl.ANY, pltpu.VMEM))
+    block_weights = [
+        array(width, 2 * shares.slot), array(width, 2 * shares.slot), array(2 * shares.slot, width),
+        sems((kinds, 8)), sems((kinds, 8)), sems((kinds, 8)), sems((kinds, 8)), sems((kinds,)),
+    ]
     return pl.pallas_call(
-        functools.partial(kernel_one, shares, width // 2),
-        out_shape=jax.ShapeDtypeStruct((half, width), jnp.bfloat16),
-        in_specs=[ANY, WHOLE, ANY, ANY, ANY],
-        out_specs=WHOLE,
+        functools.partial(layer_kernel, shares, cuts),
+        out_shape=jax.ShapeDtypeStruct(stream.shape, jnp.bfloat16),
+        in_specs=[any_space, vmem] + [any_space] * 5 + [vmem] * 4 + [any_space] * 4,
+        out_specs=any_space,
         scratch_shapes=[
-            VMEM((half, width), jnp.bfloat16), sems((1,)), sems((1,)), sems((1,)),
-        ] + ffn_scratch(half, width, shares),
-        compiler_params=params(1),
-        cost_estimate=estimate(gate_weight.shape[1], width, stream.shape[0]),
-    )(stream, gain[None], gate_weight, up_weight, down_weight)
-
-
-def second_block(first, gains, projections, mixing, weights):
-    half, width = first.shape
-    shares = Shares(weights[0].shape[1])
-    sems = pltpu.SemaphoreType.DMA
-    channels = projections[0].shape[1]
-    bf16 = jnp.bfloat16
-    return pl.pallas_call(
-        functools.partial(kernel_two, shares, width // 2),
-        out_shape=jax.ShapeDtypeStruct((2 * half, width // 2), bf16),
-        in_specs=[WHOLE, WHOLE, ANY, ANY, ANY, WHOLE, WHOLE, WHOLE, WHOLE, ANY, ANY, ANY],
-        out_specs=ANY,
-        scratch_shapes=[
-            VMEM((width, channels), bf16),
-            VMEM((width, channels), bf16),
-            VMEM(projections[2].shape, bf16),
-            VMEM((2 * half, width), bf16),
-            VMEM((2 * half, channels), bf16),
-            VMEM((2 * half, width), bf16),
-            VMEM((half, width), bf16),
-            VMEM((half, width), bf16),
-            VMEM((half, width), bf16),
-            sems((3,)), sems((3,)), sems((3,)),
-        ] + ffn_scratch(half, width, shares),
-        compiler_params=params(2),
-        cost_estimate=estimate(weights[0].shape[1], width, 2 * half),
-    )(first, gains, *projections, *mixing, *weights)
+            array(half, width), array(half, width), array(half, width), array(2 * half, width),
+            array(2 * half, channels), array(2 * half, width), array(half, width),
+            array(half, width), array(width, channels), array(width, channels),
+            array(parts, *proj_out.shape),
+            array(8 * half, width), array(8 * half, width), array(2 * half, width),
+            array(2 * half, width), array(2 * half, width), array(half, width),
+            array(half, width),
+            sems((4,)), sems((4,)), sems((1,)), sems((3, 14)), sems((3, 14)), sems((3,)),
+            sems((2, 9)), sems((2, 9)), sems((2, 3, 6)), sems((2, 3, 6)),
+        ] + block_weights + block_weights,
+        compiler_params=pltpu.CompilerParams(
+            collective_id=1, has_side_effects=True, vmem_limit_bytes=63 * 2**20
+        ),
+        cost_estimate=pl.CostEstimate(
+            flops=12 * stream.shape[0] * gate.shape[1] * width,
+            bytes_accessed=64 * gate.shape[1] * width,
+            transcendentals=0,
+        ),
+    )(*args)
 
 
 def cubes(stream, gate_weight):
@@ -641,7 +726,7 @@
         and units % (2 * LANE) == 0
         and units >= 16 * LANE
         and rows % 32 == 0
-        and width * (6 * units // 8 + 22 * stream.shape[0] // 2 + 3 * 512) * 2 < 48 * 2**20
+        and width * (12 * units // 8 + 34 * stream.shape[0] // 2 + 6 * 512) * 2 < 60 * 2**20
     )
 
 
@@ -677,14 +762,9 @@
     down_two,
 ):
     if cubes(resid, gate_one):
-        whole_u = lax.all_gather(proj_u, "fs", axis=0, tiled=True)
-        whole_v = lax.all_gather(proj_v, "fs", axis=0, tiled=True)
-        whole_out = lax.all_gather(proj_out, "fs", axis=0)
-        first = first_block(resid, norm_gains[0], gate_one, up_one, down_one)
-        return second_block(
-            first, norm_gains[1:], (whole_u, whole_v, whole_out),
-            (spatial, spatial_bias.T, mix_gain[None], head_gain[None]),
-            (gate_two, up_two, down_two),
+        return whole_layer(
+            resid, norm_gains, gate_one, up_one, down_one, proj_u, proj_v, spatial,
+            spatial_bias, mix_gain[None], head_gain[None], proj_out, gate_two, up_two, down_two,
         )
     total = feed_forward(resid, norm_gains[0], gate_one, up_one, down_one)
     first = (resid.astype(jnp.float32) + 0.5 * total).astype(jnp.bfloat16)

time: 383 us -> 300 us (0.78); the launches traced: 379 us -> 300 us
  Pallas kernels: 342 us -> 298 us
  waiting for transfers between devices: 17.9 us -> 0 us
  between operations: 13.1 us -> 0.01 us
  local copies, waits for them, and re-layouts: 6.01 us -> 1.87 us
    pallas_call x2 -> x1, Pallas kernels: 342 us -> 298 us  [whole_layer(): pl.pallas_call(functools.partial(layer_kernel, shares, cuts), out_shape=j...]
    all_gather x3 -> x0, waiting for transfers between devices: 15.8 us -> none  [the longest x1 15.7 us: body(): whole_out = lax.all_gather(proj_out, 'fs', axis=0)]
  transfers between devices with their start and end apart: 3 -> 0, of which waited for: 1 -> 0; matrix products, arithmetic and copies ran while one was open for 1% -> 0% of each run, Pallas kernels for 51% -> 0%
where the time goes in v1:
time: 300 us
  Pallas kernels  298 us (99%)
    pallas_call x1, Pallas kernels, whole_layer(): pl.pallas_call(functools.partial(layer_kernel, shares, cuts), out_shape=j...  298 us

profile of v1, /device:TPU:9, one launch (start us, length us, event | category | flops | bytes accessed | tf_op | source)
XLA Modules:
  0.0 300.2 jit_solution(12487235966132016110)
XLA Ops:
  0.0 298.3 %shard_map.145 = bf16[256,1024]{1,0:T(8,128)(2,1)} custom-call(bf16[256,1024]{1,0:T(8,128)(2,1)} %refs_0_.1, f32[3,2048]{1,0:T(4,128)} %refs_1_.1, bf16[256,2816]{1,0:T(8,128)(2,1)} %refs_2_.1, bf16[256,2816]{1,0:T(8,128)(2,1)} %refs_3_.1, bf16[2816,256]{1,0:T(8,128)(2,1)} %refs_4_.1, bf16[256,512]{1,0:T(8,128)(2,1)} %refs_5_.1, bf16[256,512]{1,0:T(8,128)(2,1)} %refs_6_.1, ...), custom_call_target="tpu_custom_call" | custom-call | flops 17716740096 | bytes 369098752 | tf_op jit(solution)/shard_map/pallas_call | solution.py:691
  298.3 1.9 copy.17

commit v2 on v1

--- a/solution.py
+++ b/solution.py
@@ -156,13 +156,16 @@
         else:
             action()
 
+    def sent(self, kind, mask):
+        return kind if kind < 3 else 3 + 7 * (kind - 3) + mask - 1
+
     def out(self, kind, mask):
         peer = xor(self.place.fs, mask)
         start, long = self.shares.of(self.place, lax.rem(peer, 4), self.place.tp)
         return long, remote(
             self.source(kind, start),
             self.target(kind, self.place.fs, self.place.tp),
-            self.send_sem.at[kind, mask],
+            self.send_sem.at[self.sent(kind, mask)],
             self.recv_sem.at[kind, mask],
             {"fs": peer},
         )
@@ -191,10 +194,22 @@
         return remote(
             target if source is None else source,
             target,
-            self.pass_send.at[kind, mask],
-            self.pass_recv.at[kind, mask],
+            self.pass_send.at[kind],
+            self.pass_recv.at[kind],
             self.place.sibling,
         )
+
+    def band(self, kind, core, owners):
+        shares, which = self.shares, kind % 3
+        first = core * shares.slot + (shares.base if kind >= 3 else 0)
+        size = shares.extra if kind >= 3 else shares.base
+        cut = pl.ds(pl.multiple_of(first, LANE), size)
+        ref = self.whole[which]
+        if which == 2:
+            band = ref.at[cut, pl.ds(0, owners * self.shards[2].shape[1])]
+        else:
+            band = ref.at[pl.ds(0, owners * self.shards[which].shape[0]), cut]
+        return band
 
     def blank(self):
         shares = self.shares
@@ -232,26 +247,30 @@
                 self.local.at[kind],
             )
             self.when(kind, long, here.wait)
-            for mask in range(8):
-                def arrived(kind=kind, mask=mask):
-                    target = self.target(kind, xor(self.place.fs, mask), 1 - self.place.tp)
-                    remote(
-                        target, target, self.pass_send.at[kind, mask],
-                        self.pass_recv.at[kind, mask], self.place.sibling,
-                    ).wait_recv()
-
-                self.when(kind, other, arrived)
+            band = self.band(kind, 1 - self.place.tp, 8)
+            passed = remote(
+                band, band, self.pass_send.at[kind], self.pass_recv.at[kind], self.place.sibling
+            )
+            self.when(kind, other, passed.wait_recv)
 
     def drain(self):
         _, long = self.shares.of(self.place, self.quarter, self.place.tp)
-        start, _ = self.shares.of(self.place, self.quarter, self.place.tp)
         for kind in range(self.kinds):
-            for mask in range(8):
-                if mask:
+            if kind >= 3:
+                for mask in range(1, 8):
                     sent, copy = self.out(kind, mask)
                     self.when(kind, sent, copy.wait_send)
-                source = self.source(kind, start) if mask == 0 else None
-                self.when(kind, long, self.passed(kind, mask, source).wait_send)
+            else:
+                band = self.band(kind, self.place.tp, 7)
+                remote(
+                    band, band, self.send_sem.at[kind], self.recv_sem.at[kind, 1],
+                    self.place.sibling,
+                ).wait_send()
+            band = self.band(kind, self.place.tp, 8)
+            passed = remote(
+                band, band, self.pass_send.at[kind], self.pass_recv.at[kind], self.place.sibling
+            )
+            self.when(kind, long, passed.wait_send)
 
 
 class Gather:
@@ -325,8 +344,8 @@
         return remote(
             self.part.at[self.block(turn, mask), columns],
             target.at[pl.ds(turn * self.half, self.half), columns],
-            self.send.at[turn, index],
-            self.recv.at[turn, index],
+            self.send.at[6 * turn + index],
+            self.recv.at[6 * turn + index],
             peer,
         )
 
@@ -350,7 +369,7 @@
 
     def z_copy(self):
         return remote(
-            self.send_z, self.from_z, self.send.at[2, 0], self.recv.at[2, 0], self.place.z_peer
+            self.send_z, self.from_z, self.send.at[12], self.recv.at[12], self.place.z_peer
         )
 
     def drain(self):
@@ -386,7 +405,7 @@
         gather.arrival(index)
 
 
-def block_sums(place, gather, weights, scatter, soon, later):
+def block_sums(place, gather, weights, scatter, soon, later, last):
     gate, up, down = weights.whole
     size = 2 * gather.half
 
@@ -419,11 +438,12 @@
     lax.fori_loop(0, 4, quadrant, jnp.int32(0))
     gather.drain()
     soon()
+    scatter.send_z[...] = scatter.total(0).astype(jnp.bfloat16)
+    scatter.z_copy().start()
     scatter.add(1, 0)
     scatter.add(1, 1)
     later()
-    scatter.send_z[...] = scatter.total(0).astype(jnp.bfloat16)
-    scatter.z_copy().start()
+    last()
     result = scatter.total(1)
     scatter.z_copy().wait_recv()
     return result + scatter.from_z[...].astype(jnp.float32)
@@ -462,7 +482,7 @@
         }[way]
         target = self.target(kind, xor(place.fs, mask), place.rep)
         source = target if mask else self.part(kind, place.rep)
-        return remote(source, target, self.send.at[kind, slot], self.recv.at[kind, slot], peer)
+        return remote(source, target, self.send.at[kind], self.recv.at[kind, slot], peer)
 
     def start(self, slots):
         for slot in slots:
@@ -478,7 +498,7 @@
             for kind in range(3):
                 target = self.target(kind, xor(place.fs, mask), half)
                 remote(
-                    target, target, self.send.at[kind, slot], self.recv.at[kind, slot],
+                    target, target, self.send.at[kind], self.recv.at[kind, slot],
                     place.x_peer,
                 ).wait_recv()
 
@@ -497,9 +517,15 @@
         return copies
 
     def drain(self):
-        for slot in range(len(self.SLOTS)):
-            for kind in range(3):
-                self.copy(kind, slot).wait_send()
+        halves = len(self.SLOTS)
+        for kind in range(3):
+            if kind == 2:
+                band = self.whole[2].at[pl.ds(0, halves // 2)]
+            else:
+                band = self.whole[kind].at[pl.ds(0, halves // 2 * self.shards[kind].shape[0]), :]
+            remote(
+                band, band, self.send.at[kind], self.recv.at[kind, 0], self.place.x_peer
+            ).wait_send()
 
 
 def mix(place, first, normed_rows, projections, mixing, gated, terms, other, send, recv):
@@ -614,10 +640,9 @@
     one.finish()
     total = block_sums(
         place, gathers[0], one, scatters[0],
-        lambda: two.start(far_pieces((1,)) + [(kind, 2) for kind in (0, 1, 2)]),
-        lambda: two.start(
-            far_pieces((2,)) + [(kind, mask) for kind in (0, 1) for mask in (1, 3)]
-        ),
+        lambda: two.start(far_pieces((1,))),
+        lambda: two.start([(kind, mask) for kind in (0, 1) for mask in (1, 3)]),
+        lambda: two.start(far_pieces((2,))),
     )
     first[...] = (mine[...].astype(jnp.float32) + 0.5 * total).astype(jnp.bfloat16)
 
@@ -639,13 +664,15 @@
     normed = rms_scale(second[...].astype(jnp.float32), gains[2:3, :])
     tokens[block, :] = normed.astype(jnp.bfloat16)
     gather_start(gathers[1])
+    one.drain()
+    mixing.drain()
     gather_near(gathers[1])
-    two.start(far_pieces(extras) + [(2, 1), (2, 3)] + near_pieces(extras))
+    two.start(far_pieces(extras) + near_pieces(extras) + [(2, 1), (2, 3), (0, 2), (1, 2), (2, 2)])
     gather_relay(gathers[1])
     two.forward(far_pieces((0, 1, 2) + extras) + near_pieces((0, 1, 2) + extras))
     gather_finish(gathers[1])
     two.finish()
-    total = block_sums(place, gathers[1], two, scatters[1], lambda: None, lambda: None)
+    total = block_sums(place, gathers[1], two, scatters[1], lambda: None, lambda: None, two.drain)
     result[...] = (second[...].astype(jnp.float32) + 0.5 * total).astype(jnp.bfloat16)
 
     last = remote(
@@ -660,9 +687,6 @@
     there.wait_send()
     trade.wait_send()
     remote(terms.at[sibling, :], other, send.at[2], recv.at[2], place.sibling).wait_send()
-    mixing.drain()
-    one.drain()
-    two.drain()
     scatters[1].drain()
     last.wait_send()
     keep.wait()
@@ -680,13 +704,15 @@
     kinds = 6 if shares.extra else 3
     parts = lax.axis_size("fs")
     even, wide = width // 2, width // 8 * 6 // LANE * LANE
-    cuts = (wide, wide, wide, even)
+    broad = width // 8 * 7 // LANE * LANE
+    cuts = (broad, wide, broad, even)
     sems = pltpu.SemaphoreType.DMA
     array = lambda *shape: VMEM(shape, jnp.bfloat16)
     any_space, vmem = (pl.BlockSpec(memory_space=space) for space in (pl.ANY, pltpu.VMEM))
     block_weights = [
         array(width, 2 * shares.slot), array(width, 2 * shares.slot), array(2 * shares.slot, width),
-        sems((kinds, 8)), sems((kinds, 8)), sems((kinds, 8)), sems((kinds, 8)), sems((kinds,)),
+        sems((3 + 7 * (kinds - 3),)), sems((kinds, 8)), sems((kinds,)), sems((kinds,)),
+        sems((kinds,)),
     ]
     return pl.pallas_call(
         functools.partial(layer_kernel, shares, cuts),
@@ -701,8 +727,8 @@
             array(8 * half, width), array(8 * half, width), array(2 * half, width),
             array(2 * half, width), array(2 * half, width), array(half, width),
             array(half, width),
-            sems((4,)), sems((4,)), sems((1,)), sems((3, 14)), sems((3, 14)), sems((3,)),
-            sems((2, 9)), sems((2, 9)), sems((2, 3, 6)), sems((2, 3, 6)),
+            sems((4,)), sems((4,)), sems((1,)), sems((3,)), sems((3, 14)), sems((3,)),
+            sems((2, 9)), sems((2, 9)), sems((2, 13)), sems((2, 13)),
         ] + block_weights + block_weights,
         compiler_params=pltpu.CompilerParams(
             collective_id=1, has_side_effects=True, vmem_limit_bytes=63 * 2**20

time: 300 us -> 287 us (0.957)
  Pallas kernels: 298 us -> 285 us
    pallas_call x1, Pallas kernels: 298 us -> 285 us  [whole_layer(): pl.pallas_call(functools.partial(layer_kernel, shares, cuts), out_shape=j...]
where the time goes in v2:
time: 287 us
  Pallas kernels  285 us (99%)
    pallas_call x1, Pallas kernels, whole_layer(): pl.pallas_call(functools.partial(layer_kernel, shares, cuts), out_shape=j...  285 us

profile of v2, /device:TPU:9, one launch (start us, length us, event | category | flops | bytes accessed | tf_op | source)
XLA Modules:
  0.0 286.9 jit_solution(6634021289548745833)
XLA Ops:
  0.0 285.0 %shard_map.145 = bf16[256,1024]{1,0:T(8,128)(2,1)} custom-call(bf16[256,1024]{1,0:T(8,128)(2,1)} %refs_0_.1, f32[3,2048]{1,0:T(4,128)} %refs_1_.1, bf16[256,2816]{1,0:T(8,128)(2,1)} %refs_2_.1, bf16[256,2816]{1,0:T(8,128)(2,1)} %refs_3_.1, bf16[2816,256]{1,0:T(8,128)(2,1)} %refs_4_.1, bf16[256,512]{1,0:T(8,128)(2,1)} %refs_5_.1, bf16[256,512]{1,0:T(8,128)(2,1)} %refs_6_.1, ...), custom_call_target="tpu_custom_call" | custom-call | flops 17716740096 | bytes 369098752 | tf_op jit(solution)/shard_map/pallas_call | solution.py:717
  285.0 1.9 copy.17
